TPU v7x, 32 devices: a whole 2x2x4 slice. The times are simulated.
32 devices in a mesh: sp: 4 (over z), tp: 4 (over y, x), dp: 2 (over core).
Axes of the slice: x: 2, y: 2, z: 4, core: 2. Of those that a mesh axis runs over, the one named last changes fastest.
Arguments:
- latent_in: bfloat16 [3072, 2048], P(('dp', 'sp', 'tp')), parts along dimension 0, may hold values from -6 to 6
- condition: bfloat16 [4096], P(('dp', 'sp')), parts along dimension 0, may hold values from -8 to 8
- context_latent: bfloat16 [1024, 256], P(('dp', 'sp')), parts along dimension 0, may hold values from -6 to 6
- context_rope: bfloat16 [1024, 64], P(('dp', 'sp')), parts along dimension 0, may hold values from -6 to 6
- shift_weight: bfloat16 [2048, 2048], P('sp', 'tp'), may hold values from -0.125 to 0.125
- scale_weight: bfloat16 [2048, 2048], P('sp', 'tp'), may hold values from -0.125 to 0.125
- gate_weight: bfloat16 [2048, 2048], P('sp', 'tp'), may hold values from -0.125 to 0.125
- norm_gain: float32 [2048], replicated, may hold values from 0.1 to 1.9
- down_query: bfloat16 [2048, 512], replicated, may hold values from -0.125 to 0.125
- down_latent: bfloat16 [2048, 256], replicated, may hold values from -0.125 to 0.125
- down_rope: bfloat16 [2048, 64], replicated, may hold values from -0.125 to 0.125
- query_gain: float32 [512], replicated, may hold values from 0.5 to 60
- latent_gain: float32 [256], replicated, may hold values from 0.1 to 1.9
- up_query: bfloat16 [512, 1536], P(None, 'tp'), may hold values from -0.25 to 0.25
- up_key: bfloat16 [256, 1024], P(None, 'tp'), may hold values from -0.375 to 0.375
- up_value: bfloat16 [256, 1024], P(None, 'tp'), may hold values from -0.375 to 0.375
- context_bias: float32 [8], P('tp'), may hold values from 1 to 2.5
- out_weight: bfloat16 [1024, 2048], replicated, may hold values from -3 to 3
Outputs:
- mixed_out: bfloat16 [3072, 2048], P(('dp', 'sp', 'tp')), parts along dimension 0
There are 2 independent parts, one for each index of `dp`. A program takes and returns all parts, laid end to end along the dimension named above; an argument that names none is the same for every part. Nothing has to cross between parts.
All inputs are finite; a program needn't handle non-finite values.
Results may differ from a plain program's by a relative error of at most 0.039.
The roundings to bfloat16 on the way count: a program that leaves them out, or rounds other values in their place, can miss the bound.
Values may be sent and summed in bfloat16 or wider, within the bound.
A program may use at most 128 MiB of HBM per device.

v0:
```python
import jax
import jax.numpy as jnp
from jax import lax
from jax.sharding import PartitionSpec as P

QK_NOPE = 128
QK_ROPE = 64
V_HEAD = 128
GRID_W = 64
epsilon = 1e-06
rope_base = 10000.0
block_limit = 2048


def rms_scaled(values, gain_vec):
    mean_sq = jnp.mean(values * values, axis=-1, keepdims=True)
    return values * lax.rsqrt(mean_sq + epsilon) * gain_vec


def rope_tables(positions, rope_width):
    freq_count = rope_width // 4
    inverse = rope_base ** (-jnp.arange(freq_count, dtype=jnp.float32) / freq_count)
    grid_row = (positions // GRID_W).astype(jnp.float32)
    grid_col = (positions % GRID_W).astype(jnp.float32)
    row_angle = grid_row[:, None] * inverse
    col_angle = grid_col[:, None] * inverse
    angles = jnp.concatenate([row_angle, row_angle, col_angle, col_angle], axis=-1)
    return (jnp.cos(angles), jnp.sin(angles))


def rope_turn(values, cosine_table, sine_table):
    part_one, part_two, part_three, part_four = jnp.split(values, 4, axis=-1)
    turned = jnp.concatenate([-part_two, part_one, -part_four, part_three], axis=-1)
    return values * cosine_table + turned * sine_table


def attend(attn_state, query_nope, query_rope, keys_nope, values_in, keys_rope, bias_col):
    score_scale = (query_nope.shape[-1] + query_rope.shape[-1]) ** (-0.5)
    scores = jnp.einsum("thd,khd->htk", query_nope, keys_nope, preferred_element_type=jnp.float32)
    scores = scores + jnp.einsum(
        "thr,kr->htk", query_rope, keys_rope, preferred_element_type=jnp.float32
    )
    scores = scores * score_scale + bias_col
    run_max, run_total, run_acc = attn_state
    new_max = jnp.maximum(run_max, jnp.max(scores, axis=-1))
    shrink = jnp.exp(run_max - new_max)
    weights = jnp.exp(scores - new_max[:, :, None])
    new_total = run_total * shrink + jnp.sum(weights, axis=-1)
    new_acc = run_acc * shrink[:, :, None] + jnp.einsum(
        "htk,khd->htd", weights.astype(jnp.bfloat16), values_in, preferred_element_type=jnp.float32
    )
    return (new_max, new_total, new_acc)


def over_blocks(attn_state, arrays, handle):
    row_count = arrays[0].shape[0]
    block_rows = 1
    for candidate in range(min(row_count, block_limit), 0, -1):
        if row_count % candidate == 0:
            block_rows = candidate
            break
    block_count = row_count // block_rows
    if block_count == 1:
        return handle(attn_state, arrays)
    stacked = tuple(
        (array_in.reshape((block_count, block_rows) + array_in.shape[1:]) for array_in in arrays)
    )

    def one_turn(inner_state, pieces):
        return (handle(inner_state, pieces), None)

    return lax.scan(one_turn, attn_state, stacked)[0]


def on_device(
    latent_in,
    condition,
    context_latent,
    context_rope,
    shift_weight,
    scale_weight,
    gate_weight,
    norm_gain,
    down_query,
    down_latent,
    down_rope,
    query_gain,
    latent_gain,
    up_query,
    up_key,
    up_value,
    context_bias,
    out_weight,
):
    activated = jax.nn.silu(condition.astype(jnp.float32)).astype(jnp.bfloat16)
    partials = jnp.stack(
        [
            jnp.dot(activated, weight_in, preferred_element_type=jnp.float32)
            for weight_in in (shift_weight, scale_weight, gate_weight)
        ]
    )
    summed = lax.psum(partials, "sp")
    modulation = lax.all_gather(summed, "tp", axis=1, tiled=True)
    shift_vec = modulation[0]
    scale_vec = modulation[1]
    gate_vec = modulation[2]
    residual_in = latent_in.astype(jnp.float32)
    normed = (rms_scaled(residual_in, norm_gain) * (1.0 + scale_vec) + shift_vec).astype(
        jnp.bfloat16
    )
    query_low = rms_scaled(
        jnp.dot(normed, down_query, preferred_element_type=jnp.float32), query_gain
    ).astype(jnp.bfloat16)
    latent_low = rms_scaled(
        jnp.dot(normed, down_latent, preferred_element_type=jnp.float32), latent_gain
    ).astype(jnp.bfloat16)
    local_rows = latent_in.shape[0]
    first_row = (lax.axis_index("sp") * lax.axis_size("tp") + lax.axis_index("tp")) * local_rows
    own_positions = first_row + jnp.arange(local_rows, dtype=jnp.int32)
    own_cosine, own_sine = rope_tables(own_positions, QK_ROPE)
    rope_keys = rope_turn(
        jnp.dot(normed, down_rope, preferred_element_type=jnp.float32), own_cosine, own_sine
    ).astype(jnp.bfloat16)
    query_group, latent_group, rope_group = (
        lax.all_gather(query_low, "tp", axis=0, tiled=True),
        lax.all_gather(latent_low, "tp", axis=0, tiled=True),
        lax.all_gather(rope_keys, "tp", axis=0, tiled=True),
    )
    group_rows = query_group.shape[0]
    group_positions = lax.axis_index("sp") * group_rows + jnp.arange(group_rows, dtype=jnp.int32)
    group_cosine, group_sine = rope_tables(group_positions, QK_ROPE)
    head_count = up_key.shape[1] // QK_NOPE
    queries = jnp.dot(query_group, up_query, preferred_element_type=jnp.float32).reshape(
        group_rows, head_count, QK_NOPE + QK_ROPE
    )
    query_nope = queries[:, :, :QK_NOPE].astype(jnp.bfloat16)
    query_rope = rope_turn(
        queries[:, :, QK_NOPE:], group_cosine[:, None, :], group_sine[:, None, :]
    ).astype(jnp.bfloat16)
    context_all, context_keys_rope = (
        lax.all_gather(context_latent, "sp", axis=0, tiled=True),
        lax.all_gather(context_rope, "sp", axis=0, tiled=True),
    )
    context_count = context_all.shape[0]
    context_nope = (
        jnp.dot(context_all, up_key, preferred_element_type=jnp.float32)
        .astype(jnp.bfloat16)
        .reshape(context_count, head_count, QK_NOPE)
    )
    context_values = (
        jnp.dot(context_all, up_value, preferred_element_type=jnp.float32)
        .astype(jnp.bfloat16)
        .reshape(context_count, head_count, V_HEAD)
    )
    start_state = (
        jnp.full((head_count, group_rows), -jnp.inf, jnp.float32),
        jnp.zeros((head_count, group_rows), jnp.float32),
        jnp.zeros((head_count, group_rows, V_HEAD), jnp.float32),
    )
    bias_col = context_bias[:, None, None]

    def context_step(inner_state, pieces):
        return attend(
            inner_state, query_nope, query_rope, pieces[0], pieces[1], pieces[2], bias_col
        )

    attn_state = over_blocks(
        start_state, (context_nope, context_values, context_keys_rope), context_step
    )
    own_nope = jnp.dot(latent_group, up_key, preferred_element_type=jnp.float32).astype(
        jnp.bfloat16
    )
    own_values = jnp.dot(latent_group, up_value, preferred_element_type=jnp.float32).astype(
        jnp.bfloat16
    )

    def expanded_step(inner_state, pieces):
        piece_rows = pieces[0].shape[0]
        return attend(
            inner_state,
            query_nope,
            query_rope,
            pieces[0].reshape(piece_rows, head_count, QK_NOPE),
            pieces[1].reshape(piece_rows, head_count, V_HEAD),
            pieces[2],
            0.0,
        )

    attn_state = over_blocks(
        attn_state,
        (
            lax.all_gather(own_nope, "sp", axis=0, tiled=True),
            lax.all_gather(own_values, "sp", axis=0, tiled=True),
            lax.all_gather(rope_group, "sp", axis=0, tiled=True),
        ),
        expanded_step,
    )
    attended = (attn_state[2] / attn_state[1][:, :, None]).astype(jnp.bfloat16)
    attended = attended.transpose(1, 0, 2).reshape(group_rows, head_count * V_HEAD)
    token_major = lax.all_to_all(attended, "tp", split_axis=0, concat_axis=1, tiled=True)
    mixed = jnp.dot(token_major, out_weight, preferred_element_type=jnp.float32)
    return (residual_in + gate_vec * mixed).astype(jnp.bfloat16)


def solution(mesh):
    in_specs = (
        P(("dp", "sp", "tp"), None),
        P(("dp", "sp")),
        P(("dp", "sp"), None),
        P(("dp", "sp"), None),
        P("sp", "tp"),
        P("sp", "tp"),
        P("sp", "tp"),
        P(),
        P(),
        P(),
        P(),
        P(),
        P(),
        P(None, "tp"),
        P(None, "tp"),
        P(None, "tp"),
        P("tp"),
        P(),
    )
    out_specs = P(("dp", "sp", "tp"), None)
    return jax.shard_map(
        on_device, mesh=mesh, in_specs=in_specs, out_specs=out_specs, check_vma=False
    )
```

profile of v0, /device:TPU:0, one launch (start us, length us, event | category | flops | bytes accessed | tf_op | source)
XLA Modules:
  0.0 158.6 jit_solution(2897633564219635338)
XLA Ops:
  0.6 0.7 fusion.54
  1.3 1.2 fusion.72
  2.6 1.2 fusion.73
  3.8 1.3 fusion.74
  5.1 13.8 %psum.7 = f32[3,512]{1,0:T(4,128)S(1)} all-reduce(f32[3,512]{1,0:T(4,128)S(1)} %pad_maximum_fusion.2), channel_id=1, replica_groups=mesh['sp'=4,'tp'=4,'dp'=2] {'sp'}, use_global_device_ids=true, to_apply=%region_0.1 | all-reduce | flops 1536 | bytes 12288 | tf_op jit(solution)/shard_map/psum | solution.py:102
  18.9 8.2 %all_gather.27 = f32[3,2048]{1,0:T(4,128)S(1)} all-gather(f32[3,512]{1,0:T(4,128)S(1)} %psum.7), channel_id=1, replica_groups=mesh['sp'=4,'tp'=4,'dp'=2] {'tp'}, dimensions={1}, use_global_device_ids=true | all-gather | bytes 30720 | tf_op jit(solution)/shard_map/all_gather | solution.py:103
  27.1 1.2 fusion.26
  28.4 1.9 %multiply_reduce_fusion.1 = (f32[96]{0:T(128)S(1)}, f32[96,256]{1,0:T(8,128)S(1)}) fusion(bf16[2048,256]{1,0:T(8,128)(2,1)} %param.27, bf16[96,2048]{1,0:T(8,128)(2,1)} %param.18, f32[2048]{0:T(1024)S(1)} %bitcast.119, f32[2048]{0:T(1024)S(1)} %bitcast.122, f32[2048]{0:T(1024)} %param.25, f32[96]{0:T(128)S(1)} %add_rsqrt_fusion.2), kind=kOutput, calls=%fused_computation.50 | convolution fusion | flops 101892000 | bytes 1565440 | tf_op jit(solution)/shard_map/dot_general | solution.py:115
  30.3 8.7 %all_gather.31 = bf16[384,256]{1,0:T(8,128)(2,1)S(1)} all-gather(bf16[96,256]{1,0:T(8,128)(2,1)S(1)} %multiply_convert_fusion.1), channel_id=1, replica_groups=mesh['sp'=4,'tp'=4,'dp'=2] {'tp'}, dimensions={0}, use_global_device_ids=true | all-gather | bytes 245760 | tf_op jit(solution)/shard_map/all_gather | solution.py:126
  39.1 13.8 %all_gather.29 = bf16[512,256]{1,0:T(8,128)(2,1)S(1)} all-gather(bf16[128,256]{1,0:T(8,128)(2,1)S(1)} %copy-done.12), channel_id=1, replica_groups=mesh['sp'=4,'tp'=4,'dp'=2] {'sp'}, dimensions={0}, use_global_device_ids=true | all-gather | bytes 327680 | tf_op jit(solution)/shard_map/all_gather | solution.py:141
  52.9 0.9 convolution_convert_fusion.3
  54.0 1.0 convolution_convert_fusion
  56.0 8.5 %all_gather.28 = bf16[384,512]{1,0:T(8,128)(2,1)S(1)} all-gather(bf16[96,512]{1,0:T(8,128)(2,1)S(1)} %multiply_convert_fusion), channel_id=1, replica_groups=mesh['sp'=4,'tp'=4,'dp'=2] {'tp'}, dimensions={0}, use_global_device_ids=true | all-gather | bytes 491520 | tf_op jit(solution)/shard_map/all_gather | solution.py:125
  65.0 0.7 slice_negate_fusion.1
  66.3 1.3 fusion.62
  67.6 0.6 copy-done.11
  68.9 0.7 broadcast_multiply_fusion.3
  69.6 0.9 fusion.47
  70.5 8.2 %all-gather = bf16[4,96,64]{1,2,0:T(8,128)(2,1)S(1)} all-gather(bf16[1,96,64]{1,2,0:T(8,128)(2,1)S(1)} %fusion.47), channel_id=1, replica_groups=mesh['sp'=4,'tp'=4,'dp'=2] {'tp'}, dimensions={0}, use_global_device_ids=true | all-gather | bytes 61440 | tf_op jit(solution)/shard_map/all_gather | solution.py:127
  78.7 0.7 copy.48
  79.4 1.6 reshape.254
  81.0 14.6 %all_gather.34 = bf16[1536,64]{0,1:T(8,128)(2,1)S(1)} all-gather(bf16[384,64]{0,1:T(8,128)(2,1)} %reshape.254), channel_id=1, replica_groups=mesh['sp'=4,'tp'=4,'dp'=2] {'sp'}, dimensions={0}, use_global_device_ids=true | all-gather | bytes 245760 | tf_op jit(solution)/shard_map/all_gather | solution.py:194
  95.6 16.9 %all_gather.32 = bf16[1536,256]{1,0:T(8,128)(2,1)S(1)} all-gather(bf16[384,256]{1,0:T(8,128)(2,1)} %convolution_convert_fusion.3), channel_id=1, replica_groups=mesh['sp'=4,'tp'=4,'dp'=2] {'sp'}, dimensions={0}, use_global_device_ids=true | all-gather | bytes 983040 | tf_op jit(solution)/shard_map/all_gather | solution.py:192
  112.9 12.2 %all_gather.30 = bf16[512,64]{0,1:T(8,128)(2,1)S(1)} all-gather(bf16[128,64]{0,1:T(8,128)(2,1)S(1)} %copy-done.13), channel_id=1, replica_groups=mesh['sp'=4,'tp'=4,'dp'=2] {'sp'}, dimensions={0}, use_global_device_ids=true | all-gather | bytes 81920 | tf_op jit(solution)/shard_map/all_gather | solution.py:142
  125.4 0.8 fusion.39
  126.3 1.0 fusion.71
  128.3 15.6 %all_gather.35 = bf16[1536,256]{1,0:T(8,128)(2,1)S(1)} all-gather(bf16[384,256]{1,0:T(8,128)(2,1)S(1)} %convolution_convert_fusion.2), channel_id=1, replica_groups=mesh['sp'=4,'tp'=4,'dp'=2] {'sp'}, dimensions={0}, use_global_device_ids=true | all-gather | bytes 983040 | tf_op jit(solution)/shard_map/all_gather | solution.py:193
  143.8 0.8 fusion.1
  144.8 0.7 fusion.19
  145.5 0.9 fusion.23
  146.8 8.1 %all_to_all.19 = bf16[4,96,256]{2,1,0:T(8,128)(2,1)S(1)} all-to-all(bf16[4,96,256]{2,1,0:T(8,128)(2,1)S(1)} %all_to_all.14), channel_id=1, replica_groups=mesh['sp'=4,'tp'=4,'dp'=2] {'tp'}, dimensions={0} | all-to-all | bytes 393216 | tf_op jit(solution)/shard_map/all_to_all | solution.py:200
  154.9 3.8 %fusion.7 = bf16[96,2048]{1,0:T(8,128)(2,1)} fusion(bf16[96,1024]{1,0:T(8,128)(2,1)S(1)} %bitcast.116, bf16[1024,2048]{1,0:T(8,128)(2,1)} %param.35, bf16[96,2048]{1,0:T(8,128)(2,1)S(1)} %copy-done.1, f32[2048]{0:T(1024)S(1)} %bitcast.118), kind=kOutput, calls=%fused_computation.9 | convolution fusion | flops 403439616 | bytes 5185536 | tf_op jit(solution)/shard_map/dot_general | solution.py:201
  (72 shorter events, 5.8 us)
Async XLA Ops:
  0.0 55.3 %copy-start = (bf16[2048,512]{1,0:T(8,128)(2,1)S(1)}, bf16[2048,512]{1,0:T(8,128)(2,1)}, u32[]{:S(2)}) copy-start(bf16[2048,512]{1,0:T(8,128)(2,1)} %param.26) | copy-start | bytes 6291460
  0.0 30.2 %copy-start.19 = (f32[256]{0:T(256)S(1)}, f32[256]{0:T(256)}, u32[]{:S(2)}) copy-start(f32[256]{0:T(256)} %param.30) | copy-start | bytes 3076
  0.0 39.0 %copy-start.12 = (bf16[128,256]{1,0:T(8,128)(2,1)S(1)}, bf16[128,256]{1,0:T(8,128)(2,1)}, u32[]{:S(2)}) copy-start(bf16[128,256]{1,0:T(8,128)(2,1)} %param.20) | copy-start | bytes 196612
  1.3 51.5 %copy-start.3 = (bf16[256,256]{1,0:T(8,128)(2,1)S(1)}, bf16[256,256]{1,0:T(8,128)(2,1)}, u32[]{:S(2)}) copy-start(bf16[256,256]{1,0:T(8,128)(2,1)} %param.32) | copy-start | bytes 393220
  3.8 50.2 %copy-start.4 = (bf16[256,256]{1,0:T(8,128)(2,1)S(1)}, bf16[256,256]{1,0:T(8,128)(2,1)}, u32[]{:S(2)}) copy-start(bf16[256,256]{1,0:T(8,128)(2,1)} %param.33) | copy-start | bytes 393220
  27.1 28.1 %copy-start.14 = (f32[1,2048]{1,0:T(1,128)}, f32[1,2048]{1,0:T(1,128)S(1)}, u32[]{:S(2)}) copy-start(f32[1,2048]{1,0:T(1,128)S(1)} %get-tuple-element.15) | copy-start | bytes 24580
  27.1 27.9 %copy-start.5 = (bf16[256,256]{1,0:T(8,128)(2,1)S(1)}, bf16[256,256]{1,0:T(8,128)(2,1)}, u32[]{:S(2)}) copy-start(bf16[256,256]{1,0:T(8,128)(2,1)} %param.33) | copy-start | bytes 393220
  28.3 26.9 %copy-start.22 = (f32[96]{0:T(128)}, f32[96]{0:T(128)S(1)}, u32[]{:S(2)}) copy-start(f32[96]{0:T(128)S(1)} %add_rsqrt_fusion.2) | copy-start | bytes 1156
  28.3 26.9 %copy-start.1 = (bf16[96,2048]{1,0:T(8,128)(2,1)S(1)}, bf16[96,2048]{1,0:T(8,128)(2,1)}, u32[]{:S(2)}) copy-start(bf16[96,2048]{1,0:T(8,128)(2,1)} %param.18) | copy-start | bytes 1179652
  28.4 26.9 %copy-start.21 = (f32[2048]{0:T(1024)S(1)}, f32[2048]{0:T(1024)}, u32[]{:S(2)}) copy-start(f32[2048]{0:T(1024)} %param.25) | copy-start | bytes 24580
  53.7 2.2 %copy-start.17 = (f32[512]{0:T(512)S(1)}, f32[512]{0:T(512)}, u32[]{:S(2)}) copy-start(f32[512]{0:T(512)} %param.29) | copy-start | bytes 6148
  54.0 10.5 %copy-start.6 = (bf16[512,384]{1,0:T(8,128)(2,1)S(1)}, bf16[512,384]{1,0:T(8,128)(2,1)}, u32[]{:S(2)}) copy-start(bf16[512,384]{1,0:T(8,128)(2,1)} %param.31) | copy-start | bytes 1179652
  67.6 0.6 copy-start.11
  70.5 54.6 %copy-start.15 = (f32[384]{0:T(512)S(1)}, f32[384]{0:T(512)}, u32[]{:S(2)}) copy-start(f32[384]{0:T(512)} %get-tuple-element.33) | copy-start | bytes 4612
  70.5 54.6 %copy-start.16 = (f32[384]{0:T(512)S(1)}, f32[384]{0:T(512)}, u32[]{:S(2)}) copy-start(f32[384]{0:T(512)} %get-tuple-element.34) | copy-start | bytes 4612
  81.0 31.9 %copy-start.13 = (bf16[128,64]{0,1:T(8,128)(2,1)S(1)}, bf16[128,64]{0,1:T(8,128)(2,1)}, u32[]{:S(2)}) copy-start(bf16[128,64]{0,1:T(8,128)(2,1)} %param.21) | copy-start | bytes 49156
  81.0 44.1 %copy-start.18 = (f32[16]{0:T(128)S(1)}, f32[16]{0:T(128)}, u32[]{:S(2)}) copy-start(f32[16]{0:T(128)} %multiply_power_fusion) | copy-start | bytes 196
  81.0 44.4 %copy-start.7 = (f32[384,2,16]{0,2,1:T(8,128)S(1)}, f32[384,2,16]{0,2,1:T(8,128)}, u32[]{:S(2)}) copy-start(f32[384,2,16]{0,2,1:T(8,128)} %get-tuple-element.7) | copy-start | bytes 147460
  81.0 44.4 %copy-start.8 = (f32[384,2,16]{0,2,1:T(8,128)S(1)}, f32[384,2,16]{0,2,1:T(8,128)}, u32[]{:S(2)}) copy-start(f32[384,2,16]{0,2,1:T(8,128)} %get-tuple-element.8) | copy-start | bytes 147460
  81.0 44.4 %copy-start.9 = (f32[384,2,16]{0,2,1:T(8,128)S(1)}, f32[384,2,16]{0,2,1:T(8,128)}, u32[]{:S(2)}) copy-start(f32[384,2,16]{0,2,1:T(8,128)} %get-tuple-element.9) | copy-start | bytes 147460
  81.0 44.4 %copy-start.10 = (f32[384,2,16]{0,2,1:T(8,128)S(1)}, f32[384,2,16]{0,2,1:T(8,128)}, u32[]{:S(2)}) copy-start(f32[384,2,16]{0,2,1:T(8,128)} %get-tuple-element.10) | copy-start | bytes 147460
  126.3 1.0 copy-start.20
  143.8 1.0 copy-start.2
where the time goes:
time: 159 us
  blocking collectives  129 us (81%)
  matrix products  18.4 us (12%)
  other arithmetic  7.9 us (5%)
  local copies, waits for them, and re-layouts  3.43 us (2%)
    all_gather x1, blocking collectives, on_device(): lax.all_gather(own_nope, 'sp', axis=0, tiled=True)  16.9 us
    all_gather x1, blocking collectives, on_device(): lax.all_gather(own_values, 'sp', axis=0, tiled=True)  15.6 us
    all_gather x1, blocking collectives, on_device(): lax.all_gather(rope_group, 'sp', axis=0, tiled=True)  14.6 us
    all_gather x1, blocking collectives, on_device(): lax.all_gather(context_latent, 'sp', axis=0, tiled=True)  13.8 us
    psum x1, blocking collectives, on_device(): summed = lax.psum(partials, 'sp')  13.8 us
    all_gather x1, blocking collectives, on_device(): lax.all_gather(context_rope, 'sp', axis=0, tiled=True)  12.2 us
    all_gather x1, blocking collectives, on_device(): lax.all_gather(latent_low, 'tp', axis=0, tiled=True)  8.7 us
    all_gather x1, blocking collectives, on_device(): lax.all_gather(query_low, 'tp', axis=0, tiled=True)  8.53 us

commit v1 on v0

--- a/solution.py
+++ b/solution.py
@@ -99,7 +99,10 @@
             for weight_in in (shift_weight, scale_weight, gate_weight)
         ]
     )
-    summed = lax.psum(partials, "sp")
+    devices, summed = (lax.axis_size("sp"), partials)
+    for far in [1 << k for k in range(devices.bit_length() - 1)]:
+        route = [(i, i ^ far) for i in range(devices)]
+        summed = summed + lax.ppermute(summed, "sp", route)
     modulation = lax.all_gather(summed, "tp", axis=1, tiled=True)
     shift_vec = modulation[0]
     scale_vec = modulation[1]

time: 159 us -> 148 us (0.931)
  blocking collectives: 129 us -> 118 us
  starting transfers between devices: 0 us -> 3.84 us
  other arithmetic: 7.9 us -> 5.42 us
    psum x1 -> x0, blocking collectives: 13.8 us -> none  [on_device(): summed = lax.psum(partials, 'sp')]
    ppermute x0 -> x2, starting transfers between devices: none -> 3.84 us  [on_device(): summed = summed + lax.ppermute(summed, 'sp', route)]
  transfers between devices with their start and end apart: 0 -> 2, of which waited for: 0 -> 0; matrix products, arithmetic and copies ran while one was open for 0% -> 2% of each run, Pallas kernels for 0% -> 0%
where the time goes in v1:
time: 148 us
  blocking collectives  118 us (80%)
  matrix products  17.2 us (12%)
  other arithmetic  5.42 us (4%)
  starting transfers between devices  3.84 us (3%)
  local copies, waits for them, and re-layouts  2.8 us (2%)
    all_gather x1, blocking collectives, on_device(): lax.all_gather(own_nope, 'sp', axis=0, tiled=True)  18.1 us
    all_gather x1, blocking collectives, on_device(): lax.all_gather(own_values, 'sp', axis=0, tiled=True)  15.7 us
    all_gather x1, blocking collectives, on_device(): lax.all_gather(rope_group, 'sp', axis=0, tiled=True)  14.6 us
    all_gather x1, blocking collectives, on_device(): lax.all_gather(context_latent, 'sp', axis=0, tiled=True)  14.3 us
    all_gather x1, blocking collectives, on_device(): lax.all_gather(context_rope, 'sp', axis=0, tiled=True)  12.6 us
    all_gather x1, blocking collectives, on_device(): lax.all_gather(latent_low, 'tp', axis=0, tiled=True)  9.45 us
    all_gather x1, blocking collectives, on_device(): lax.all_gather(rope_keys, 'tp', axis=0, tiled=True)  8.84 us
    all_gather x1, blocking collectives, on_device(): modulation = lax.all_gather(summed, 'tp', axis=1, tiled=True)  8.2 us
  transfers between devices with their start and end apart: 2, of which 0 were waited for; matrix products, arithmetic and copies ran while one was open for 2% of the time, Pallas kernels for 0%

profile of v1, /device:TPU:0, one launch (start us, length us, event | category | flops | bytes accessed | tf_op | source)
XLA Modules:
  0.0 147.6 jit_solution(17192571535624305825)
XLA Ops:
  0.0 0.8 fusion.53
  0.9 1.3 fusion.72
  2.1 1.2 fusion.73
  3.4 1.2 fusion.74
  4.6 3.1 %collective-permute-start = (f32[3,512]{1,0:T(4,128)S(1)}, f32[3,512]{1,0:T(4,128)S(1)}, u32[]{:S(2)}, u32[]{:S(2)}) collective-permute-start(f32[3,512]{1,0:T(4,128)S(1)} %pad_maximum_fusion.2), channel_id=1, source_target_pairs={{0,8},{8,0},{16,24},{24,16},{1,9},{9,1},{17,25},{25,17},{2,10},{10... | collective-permute-start | bytes 18440 | tf_op jit(solution)/shard_map/ppermute | solution.py:105
  7.7 1.2 fusion.24
  9.0 14.3 %all_gather.29 = bf16[512,256]{1,0:T(8,128)(2,1)S(1)} all-gather(bf16[128,256]{1,0:T(8,128)(2,1)} %param.20), channel_id=1, replica_groups=mesh['sp'=4,'tp'=4,'dp'=2] {'sp'}, dimensions={0}, use_global_device_ids=true | all-gather | bytes 327680 | tf_op jit(solution)/shard_map/all_gather | solution.py:144
  23.6 1.0 convolution_convert_fusion
  24.7 0.9 fusion.41
  25.6 0.7 collective-permute-start.1
  26.3 12.6 %all_gather.30 = bf16[512,64]{0,1:T(8,128)(2,1)} all-gather(bf16[128,64]{0,1:T(8,128)(2,1)S(1)} %copy-done.13), channel_id=1, replica_groups=mesh['sp'=4,'tp'=4,'dp'=2] {'sp'}, dimensions={0}, use_global_device_ids=true | all-gather | bytes 81920 | tf_op jit(solution)/shard_map/all_gather | solution.py:145
  38.9 8.2 %all_gather.27 = f32[3,2048]{1,0:T(4,128)S(1)} all-gather(f32[3,512]{1,0:T(4,128)S(1)} %fusion.101), channel_id=1, replica_groups=mesh['sp'=4,'tp'=4,'dp'=2] {'tp'}, dimensions={1}, use_global_device_ids=true | all-gather | bytes 30720 | tf_op jit(solution)/shard_map/all_gather | solution.py:106
  47.2 1.7 %multiply_reduce_fusion.1 = (f32[96]{0:T(128)S(1)}, f32[96,256]{1,0:T(8,128)S(1)}) fusion(bf16[2048,256]{1,0:T(8,128)(2,1)} %param.27, bf16[96,2048]{1,0:T(8,128)(2,1)S(1)} %copy-done.1, f32[2048]{0:T(1024)S(1)} %bitcast.119, f32[2048]{0:T(1024)S(1)} %bitcast.122, f32[2048]{0:T(1024)S(1)} %copy-done.18, f32[96]{0:T(128)S(1)} %add_rsqrt_fusion.2), kind=kOutput, calls=%fused_computation.49 | convolution fusion | flops 101892000 | bytes 1565440 | tf_op jit(solution)/shard_map/dot_general | solution.py:118
  49.0 9.4 %all_gather.31 = bf16[384,256]{1,0:T(8,128)(2,1)S(1)} all-gather(bf16[96,256]{1,0:T(8,128)(2,1)S(1)} %multiply_convert_fusion.1), channel_id=1, replica_groups=mesh['sp'=4,'tp'=4,'dp'=2] {'tp'}, dimensions={0}, use_global_device_ids=true | all-gather | bytes 245760 | tf_op jit(solution)/shard_map/all_gather | solution.py:129
  58.4 0.9 convolution_convert_fusion.3
  59.6 0.6 multiply_reduce_fusion
  60.3 8.1 %all_gather.28 = bf16[384,512]{1,0:T(8,128)(2,1)S(1)} all-gather(bf16[96,512]{1,0:T(8,128)(2,1)S(1)} %multiply_convert_fusion), channel_id=1, replica_groups=mesh['sp'=4,'tp'=4,'dp'=2] {'tp'}, dimensions={0}, use_global_device_ids=true | all-gather | bytes 491520 | tf_op jit(solution)/shard_map/all_gather | solution.py:128
  68.8 0.7 slice_negate_fusion.1
  70.0 8.8 %all-gather = bf16[4,96,64]{1,2,0:T(8,128)(2,1)S(1)} all-gather(bf16[1,96,64]{1,2,0:T(8,128)(2,1)S(1)} %fusion.46), channel_id=1, replica_groups=mesh['sp'=4,'tp'=4,'dp'=2] {'tp'}, dimensions={0}, use_global_device_ids=true | all-gather | bytes 61440 | tf_op jit(solution)/shard_map/all_gather | solution.py:130
  78.8 0.7 copy.48
  79.5 1.6 %reshape.254 = bf16[384,64]{0,1:T(8,128)(2,1)} reshape(bf16[4,96,64]{1,0,2:T(4,128)(2,1)} %copy.48) | data formatting | bytes 98304
  81.1 14.6 %all_gather.34 = bf16[1536,64]{0,1:T(8,128)(2,1)S(1)} all-gather(bf16[384,64]{0,1:T(8,128)(2,1)} %reshape.254), channel_id=1, replica_groups=mesh['sp'=4,'tp'=4,'dp'=2] {'sp'}, dimensions={0}, use_global_device_ids=true | all-gather | bytes 245760 | tf_op jit(solution)/shard_map/all_gather | solution.py:197
  95.7 18.1 %all_gather.32 = bf16[1536,256]{1,0:T(8,128)(2,1)S(1)} all-gather(bf16[384,256]{1,0:T(8,128)(2,1)} %convolution_convert_fusion.3), channel_id=1, replica_groups=mesh['sp'=4,'tp'=4,'dp'=2] {'sp'}, dimensions={0}, use_global_device_ids=true | all-gather | bytes 983040 | tf_op jit(solution)/shard_map/all_gather | solution.py:195
  114.4 0.8 fusion.38
  115.2 1.0 fusion.71
  116.2 0.5 fusion.70
  117.2 15.7 %all_gather.35 = bf16[1536,256]{1,0:T(8,128)(2,1)S(1)} all-gather(bf16[384,256]{1,0:T(8,128)(2,1)S(1)} %convolution_convert_fusion.2), channel_id=1, replica_groups=mesh['sp'=4,'tp'=4,'dp'=2] {'sp'}, dimensions={0}, use_global_device_ids=true | all-gather | bytes 983040 | tf_op jit(solution)/shard_map/all_gather | solution.py:196
  132.9 0.8 fusion.1
  133.8 0.7 fusion.17
  134.5 0.9 fusion.21
  135.8 8.1 %all_to_all.19 = bf16[4,96,256]{2,1,0:T(8,128)(2,1)S(1)} all-to-all(bf16[4,96,256]{2,1,0:T(8,128)(2,1)S(1)} %all_to_all.14), channel_id=1, replica_groups=mesh['sp'=4,'tp'=4,'dp'=2] {'tp'}, dimensions={0} | all-to-all | bytes 393216 | tf_op jit(solution)/shard_map/all_to_all | solution.py:203
  143.9 3.8 %fusion.29 = bf16[96,2048]{1,0:T(8,128)(2,1)} fusion(bf16[96,2048]{1,0:T(8,128)(2,1)S(1)} %copy-done.1, f32[2048]{0:T(1024)S(1)} %bitcast.118, bf16[96,1024]{1,0:T(8,128)(2,1)S(1)} %bitcast.116, bf16[1024,2048]{1,0:T(8,128)(2,1)} %param.35), kind=kOutput, calls=%fused_computation.32 | convolution fusion | flops 403439616 | bytes 5185536 | tf_op jit(solution)/shard_map/dot_general | solution.py:204
  (73 shorter events, 3.3 us)
Async XLA Ops:
  0.0 59.6 %copy-start = (bf16[2048,512]{1,0:T(8,128)(2,1)S(1)}, bf16[2048,512]{1,0:T(8,128)(2,1)}, u32[]{:S(2)}) copy-start(bf16[2048,512]{1,0:T(8,128)(2,1)} %param.26) | copy-start | bytes 6291460
  0.0 47.2 %copy-start.1 = (bf16[96,2048]{1,0:T(8,128)(2,1)S(1)}, bf16[96,2048]{1,0:T(8,128)(2,1)}, u32[]{:S(2)}) copy-start(bf16[96,2048]{1,0:T(8,128)(2,1)} %param.18) | copy-start | bytes 1179652
  0.0 23.3 %copy-start.3 = (bf16[256,256]{1,0:T(8,128)(2,1)S(1)}, bf16[256,256]{1,0:T(8,128)(2,1)}, u32[]{:S(2)}) copy-start(bf16[256,256]{1,0:T(8,128)(2,1)} %param.32) | copy-start | bytes 393220
  0.0 23.6 %copy-start.4 = (bf16[256,256]{1,0:T(8,128)(2,1)S(1)}, bf16[256,256]{1,0:T(8,128)(2,1)}, u32[]{:S(2)}) copy-start(bf16[256,256]{1,0:T(8,128)(2,1)} %param.33) | copy-start | bytes 393220
  0.0 26.3 %copy-start.13 = (bf16[128,64]{0,1:T(8,128)(2,1)S(1)}, bf16[128,64]{0,1:T(8,128)(2,1)}, u32[]{:S(2)}) copy-start(bf16[128,64]{0,1:T(8,128)(2,1)} %param.21) | copy-start | bytes 49156
  0.0 47.2 %copy-start.18 = (f32[2048]{0:T(1024)S(1)}, f32[2048]{0:T(1024)}, u32[]{:S(2)}) copy-start(f32[2048]{0:T(1024)} %param.25) | copy-start | bytes 24580
  4.6 44.3 %copy-start.15 = (f32[256]{0:T(256)S(1)}, f32[256]{0:T(256)}, u32[]{:S(2)}) copy-start(f32[256]{0:T(256)} %param.30) | copy-start | bytes 3076
  4.6 21.0 %collective-permute-start = (f32[3,512]{1,0:T(4,128)S(1)}, f32[3,512]{1,0:T(4,128)S(1)}, u32[]{:S(2)}, u32[]{:S(2)}) collective-permute-start(f32[3,512]{1,0:T(4,128)S(1)} %pad_maximum_fusion.2), channel_id=1, source_target_pairs={{0,8},{8,0},{16,24},{24,16},{1,9},{9,1},{17,25},{25,17},{2,10},{10... | collective-permute-start | bytes 18440 | tf_op jit(solution)/shard_map/ppermute | solution.py:105
  8.9 50.6 %copy-start.19 = (f32[96]{0:T(128)}, f32[96]{0:T(128)S(1)}, u32[]{:S(2)}) copy-start(f32[96]{0:T(128)S(1)} %add_rsqrt_fusion.2) | copy-start | bytes 1156
  25.6 13.3 %collective-permute-start.1 = (f32[3,512]{1,0:T(4,128)S(1)}, f32[3,512]{1,0:T(4,128)S(1)}, u32[]{:S(2)}, u32[]{:S(2)}) collective-permute-start(f32[3,512]{1,0:T(4,128)S(1)} %fusion.61), channel_id=1, source_target_pairs={{0,16},{8,24},{16,0},{24,8},{1,17},{9,25},{17,1},{25,9},{2,18},{10... | collective-permute-start | bytes 18440 | tf_op jit(solution)/shard_map/ppermute | solution.py:105
  48.9 11.3 %copy-start.14 = (f32[512]{0:T(512)S(1)}, f32[512]{0:T(512)}, u32[]{:S(2)}) copy-start(f32[512]{0:T(512)} %param.29) | copy-start | bytes 6148
  58.4 10.0 %copy-start.5 = (bf16[512,384]{1,0:T(8,128)(2,1)S(1)}, bf16[512,384]{1,0:T(8,128)(2,1)}, u32[]{:S(2)}) copy-start(bf16[512,384]{1,0:T(8,128)(2,1)} %param.31) | copy-start | bytes 1179652
  59.6 9.9 %copy-start.17 = (bf16[2048,64]{0,1:T(8,128)(2,1)S(1)}, bf16[2048,64]{0,1:T(8,128)(2,1)}, u32[]{:S(2)}) copy-start(bf16[2048,64]{0,1:T(8,128)(2,1)} %param.28) | copy-start | bytes 786436
  60.2 9.3 %copy-start.20 = (f32[96]{0:T(128)S(1)}, f32[96]{0:T(128)}, u32[]{:S(2)}) copy-start(f32[96]{0:T(128)} %copy-done.19) | copy-start | bytes 1156
  81.1 33.2 %copy-start.6 = (f32[384,64]{0,1:T(8,128)S(1)}, f32[384,64]{0,1:T(8,128)}, u32[]{:S(2)}) copy-start(f32[384,64]{0,1:T(8,128)} %get-tuple-element.11) | copy-start | bytes 294916
  81.1 33.2 %copy-start.7 = (f32[384,64]{0,1:T(8,128)S(1)}, f32[384,64]{0,1:T(8,128)}, u32[]{:S(2)}) copy-start(f32[384,64]{0,1:T(8,128)} %get-tuple-element.12) | copy-start | bytes 294916
  81.1 33.2 %copy-start.9 = (f32[384,2,16]{0,2,1:T(8,128)S(1)}, f32[384,2,16]{0,2,1:T(8,128)}, u32[]{:S(2)}) copy-start(f32[384,2,16]{0,2,1:T(8,128)} %get-tuple-element.7) | copy-start | bytes 147460
  81.1 33.2 %copy-start.10 = (f32[384,2,16]{0,2,1:T(8,128)S(1)}, f32[384,2,16]{0,2,1:T(8,128)}, u32[]{:S(2)}) copy-start(f32[384,2,16]{0,2,1:T(8,128)} %get-tuple-element.8) | copy-start | bytes 147460
  81.1 33.2 %copy-start.11 = (f32[384,2,16]{0,2,1:T(8,128)S(1)}, f32[384,2,16]{0,2,1:T(8,128)}, u32[]{:S(2)}) copy-start(f32[384,2,16]{0,2,1:T(8,128)} %get-tuple-element.9) | copy-start | bytes 147460
  81.1 33.2 %copy-start.12 = (f32[384,2,16]{0,2,1:T(8,128)S(1)}, f32[384,2,16]{0,2,1:T(8,128)}, u32[]{:S(2)}) copy-start(f32[384,2,16]{0,2,1:T(8,128)} %get-tuple-element.10) | copy-start | bytes 147460
  115.2 1.0 copy-start.8
  115.2 1.0 copy-start.16
  132.9 1.0 copy-start.2
